TPU v7x, 256 devices: a whole 4x4x8 slice. The times are simulated.
256 devices in a mesh: ep: 16 (over y, x), tp: 16 (over z, core).
Axes of the slice: x: 4, y: 4, z: 8, core: 2. Of those that a mesh axis runs over, the one named last changes fastest.
Arguments:
- tokens: bfloat16 [256, 2048], P('ep', 'tp'), may hold values from -6 to 6
- key_cache: bfloat16 [256, 16, 1024, 128], P('ep', 'tp'), may hold values from -1700 to 1700
- value_cache: bfloat16 [256, 16, 1024, 128], P('ep', 'tp'), may hold values from -6 to 6
- gate_totals: float32 [256, 16, 1024], P('ep', 'tp'), as said below
- lengths: int32 [256], P('ep'), may hold values from 128 to 1024
- attn_gain: float32 [2048], replicated, may hold values from 0.1 to 1.9
- w_query: bfloat16 [2048, 2048], P(None, 'tp'), may hold values from -0.125 to 0.125
- w_key: bfloat16 [2048, 2048], P(None, 'tp'), may hold values from -0.125 to 0.125
- w_value: bfloat16 [2048, 2048], P(None, 'tp'), may hold values from -0.125 to 0.125
- w_forget: bfloat16 [2048, 16], replicated, may hold values from -0.125 to 0.125
- forget_bias: float32 [16], replicated, may hold values from -3 to 0
- w_attn_out: bfloat16 [2048, 2048], P('tp'), may hold values from -0.1875 to 0.1875
- moe_gain: float32 [2048], replicated, may hold values from 0.1 to 1.9
- group_ids: int32 [256, 1], P('ep'), may hold values from 0 to 15; in each aligned block of 16 rows (0 to 15, 16 to 31, ...) at most 2 rows name the same one
- inner_ids: int32 [256, 2], P('ep'), may hold values from 0 to 3, all different within a row
- group_prob: float32 [256], P('ep'), may hold values from 0.2 to 1
- pair_logits: float32 [256, 2], P('ep'), may hold values from -6 to 6
- w_expert_gate: bfloat16 [16, 2048, 2048], P('ep', None, 'tp'), may hold values from -0.125 to 0.125
- w_expert_up: bfloat16 [16, 2048, 2048], P('ep', None, 'tp'), may hold values from -0.125 to 0.125
- w_expert_down: bfloat16 [16, 2048, 2048], P('ep', 'tp'), may hold values from -0.375 to 0.375
- w_dense_in: bfloat16 [2048, 2048], P(None, 'tp'), may hold values from -0.125 to 0.125
- w_dense_out: bfloat16 [2048, 2048], P('tp'), may hold values from -0.1875 to 0.1875
- dense_gate: float32 [2048], P('tp'), may hold values from -2 to 2
Outputs:
- layer_output: bfloat16 [256, 2048], P('ep', 'tp')
- new_keys: bfloat16 [256, 16, 128], P('ep', 'tp')
- new_values: bfloat16 [256, 16, 128], P('ep', 'tp')
- new_gates: float32 [256, 16], P('ep', 'tp')
Inputs may be any that keep to these rules, and one draw needn't show every extreme that they name: `group_ids`: within the 16 sequences of each index of ep (aligned blocks of rows), no group is named by more than 2 sequences, a bound that some block reaches. `inner_ids`: each row names 2 different experts of its group. `gate_totals`: along positions the values of each sequence and head never rise.
All inputs are finite; a program needn't handle non-finite values.
Results may differ from a plain program's by a relative error of at most 0.011.
Values may be sent and summed in bfloat16 or wider, within the bound.
A program may use at most 64 MiB of HBM per device.

v0:
```python
import jax
import jax.numpy as jnp
from jax import lax
from jax.sharding import PartitionSpec as P

FFE = 512
EPG = 4
EPS = 1e-06
FLOOR = -1e30


def split_up(array, dim, size):
    dims = array.shape
    pieces = array.reshape(*dims[:dim], size, dims[dim] // size, *dims[dim + 1 :])
    return jnp.moveaxis(pieces, dim, 0)


def sum_at_owner(array, axis, dim):
    size = lax.axis_size(axis)
    pieces = lax.all_to_all(split_up(array, dim, size), axis, 0, 0, tiled=True)
    return jnp.sum(pieces, axis=0)


def joined_along(pieces, dim):
    dims = list(pieces.shape[1:])
    dims[dim] *= pieces.shape[0]
    return jnp.moveaxis(pieces, 0, dim).reshape(dims)


def copy_for_each(array, axis):
    copies = jnp.broadcast_to(array, (lax.axis_size(axis), *array.shape))
    return lax.all_to_all(copies, axis, split_axis=0, concat_axis=0, tiled=True)


def gathered_copies(array, axis, dim):
    return joined_along(copy_for_each(array, axis), dim)


def side_by_side(arrays, axis, split_dim, concat_dim, along):
    both = jnp.concatenate(arrays, axis=along)
    filled, at, gathered = (
        lax.all_to_all(both, axis, split_axis=split_dim, concat_axis=concat_dim, tiled=True),
        0,
        [],
    )
    for a in arrays:
        gathered.append(lax.slice_in_dim(filled, at, at + a.shape[along], axis=along))
        at += a.shape[along]
    return tuple(gathered)


def sent_together(arrays, axis, dim, along):
    widths = [a.shape[along] for a in arrays]
    both = jnp.concatenate(arrays, axis=along)
    filled = sum_at_owner(both, axis, dim)
    return tuple(jnp.split(filled, [sum(widths[:k]) for k in range(1, len(widths))], axis=along))


def norm_rows(row_data, gain_vec):
    values = row_data.astype(jnp.float32)
    factor = lax.rsqrt(jnp.mean(values * values, axis=-1, keepdims=True) + EPS)
    return (values * factor * gain_vec).astype(jnp.bfloat16)


def head_norm(values):
    factor = lax.rsqrt(jnp.mean(values * values, axis=-1, keepdims=True) + EPS)
    return (values * factor).astype(jnp.bfloat16)


def attend(queries, fresh_key, fresh_value, key_cache, value_cache, gate_totals, lengths, current):
    score_scale = queries.shape[-1] ** (-0.5)
    scores = (
        jnp.einsum("shd,shld->shl", queries, key_cache, preferred_element_type=jnp.float32)
        * score_scale
    )
    scores = scores + current[:, :, None] - gate_totals
    entry_indices = jnp.arange(key_cache.shape[2])
    live_mask = (entry_indices[None, :] < lengths[:, None])[:, None, :]
    scores = jnp.where(live_mask, scores, FLOOR)
    own_score = (
        jnp.sum(queries.astype(jnp.float32) * fresh_key.astype(jnp.float32), axis=-1) * score_scale
    )
    peak = jnp.maximum(jnp.max(scores, axis=-1), own_score)
    expo_terms = jnp.where(live_mask, jnp.exp(scores - peak[:, :, None]), 0.0)
    own_expo = jnp.exp(own_score - peak)
    denom_sum = jnp.sum(expo_terms, axis=-1) + own_expo
    weights = (expo_terms / denom_sum[:, :, None]).astype(jnp.bfloat16)
    own_weight = (own_expo / denom_sum).astype(jnp.bfloat16)
    attended = jnp.einsum("shl,shld->shd", weights, value_cache, preferred_element_type=jnp.float32)
    attended = attended + own_weight.astype(jnp.float32)[:, :, None] * fresh_value.astype(
        jnp.float32
    )
    return attended.astype(jnp.bfloat16)


def body(
    tokens,
    key_cache,
    value_cache,
    gate_totals,
    lengths,
    attn_gain,
    w_query,
    w_key,
    w_value,
    w_forget,
    forget_bias,
    w_attn_out,
    moe_gain,
    group_ids,
    inner_ids,
    group_prob,
    pair_logits,
    w_expert_gate,
    w_expert_up,
    w_expert_down,
    w_dense_in,
    w_dense_out,
    dense_gate,
):
    gathered = lax.all_gather(tokens, "tp", axis=1, tiled=True)
    normed = norm_rows(gathered, attn_gain)
    seq_count = gathered.shape[0]
    heads_dev = key_cache.shape[1]
    head_dim = key_cache.shape[3]

    def project(weight):
        return jnp.dot(normed, weight, preferred_element_type=jnp.float32).reshape(
            seq_count, heads_dev, head_dim
        )

    queries = head_norm(project(w_query))
    new_keys = head_norm(project(w_key))
    new_values = project(w_value).astype(jnp.bfloat16)
    first_head = lax.axis_index("tp") * heads_dev
    forget_cols = lax.dynamic_slice_in_dim(w_forget, first_head, heads_dev, 1)
    forget_shift = lax.dynamic_slice_in_dim(forget_bias, first_head, heads_dev, 0)
    log_gate = jax.nn.log_sigmoid(
        jnp.dot(normed, forget_cols, preferred_element_type=jnp.float32) + forget_shift
    )
    entry_indices = jnp.arange(gate_totals.shape[2])
    at_last = (entry_indices[None, :] == (lengths - 1)[:, None])[:, None, :]
    new_gates = jnp.sum(jnp.where(at_last, gate_totals, 0.0), axis=2) + log_gate
    attended = attend(
        queries, new_keys, new_values, key_cache, value_cache, gate_totals, lengths, new_gates
    )
    partial_value = jnp.dot(
        attended.reshape(seq_count, heads_dev * head_dim),
        w_attn_out,
        preferred_element_type=jnp.float32,
    )
    piece_sum = sum_at_owner(partial_value, "tp", 1)
    own_residual = (tokens.astype(jnp.float32) + piece_sum).astype(jnp.bfloat16)
    moe_in = norm_rows(gathered_copies(own_residual, "tp", 1), moe_gain)
    groups = lax.axis_size("ep")
    capacity = max(2, 2 * seq_count // groups)
    first_share = jax.nn.sigmoid(pair_logits[:, 0] - pair_logits[:, 1])
    pair_share = group_prob[:, None] * jnp.stack([first_share, 1.0 - first_share], axis=1)
    inner_range = jnp.arange(EPG)
    spread = jnp.sum(
        jnp.where(inner_ids[:, :, None] == inner_range[None, None, :], pair_share[:, :, None], 0.0),
        axis=1,
    ).astype(jnp.bfloat16)
    choose = (group_ids == jnp.arange(groups)[None, :]).astype(jnp.int32)
    before = jnp.cumsum(choose, axis=0) - choose
    slot_of = group_ids[:, 0] * capacity + jnp.sum(before * choose, axis=1)
    slot_ids = jnp.arange(groups * capacity)
    send_map = (slot_of[None, :] == slot_ids[:, None]).astype(jnp.bfloat16)
    send_weights = jnp.dot(send_map, spread, preferred_element_type=jnp.float32).astype(
        jnp.bfloat16
    )
    send_rows = jnp.dot(send_map, moe_in, preferred_element_type=jnp.float32).astype(jnp.bfloat16)
    recv_rows, recv_weights = side_by_side((send_rows, send_weights), "ep", 0, 0, 1)
    dense_hidden = jax.nn.silu(
        jnp.dot(moe_in, w_dense_in, preferred_element_type=jnp.float32)
    ).astype(jnp.bfloat16)
    dense_part = jnp.dot(dense_hidden, w_dense_out, preferred_element_type=jnp.float32)
    hidden_dev = w_expert_gate.shape[2]
    expert_index = lax.axis_index("tp") * hidden_dev // FFE
    route_col = jnp.sum(
        jnp.where(inner_range[None, :] == expert_index, recv_weights.astype(jnp.float32), 0.0),
        axis=1,
    )
    gate_pre = jnp.dot(recv_rows, w_expert_gate[0], preferred_element_type=jnp.float32)
    up_pre = jnp.dot(recv_rows, w_expert_up[0], preferred_element_type=jnp.float32)
    hidden = (jax.nn.silu(gate_pre) * up_pre * route_col[:, None]).astype(jnp.bfloat16)
    expert_part = jnp.dot(hidden, w_expert_down[0], preferred_element_type=jnp.float32)
    expert_sum, dense_sum = sent_together((expert_part, dense_part), "tp", 1, 0)
    returned = lax.all_to_all(
        expert_sum.astype(jnp.bfloat16), "ep", split_axis=0, concat_axis=0, tiled=True
    )
    expert_out = lax.dot_general(
        send_map, returned, (((0,), (0,)), ((), ())), preferred_element_type=jnp.float32
    )
    layer_output = (
        own_residual.astype(jnp.float32) + expert_out + jax.nn.sigmoid(dense_gate) * dense_sum
    )
    return (layer_output.astype(jnp.bfloat16), new_keys, new_values, new_gates)


def solution(mesh):
    placed = (
        P("ep", "tp"),
        P("ep", "tp", None, None),
        P("ep", "tp", None, None),
        P("ep", "tp", None),
        P("ep"),
        P(),
        P(None, "tp"),
        P(None, "tp"),
        P(None, "tp"),
        P(),
        P(),
        P("tp", None),
        P(),
        P("ep", None),
        P("ep", None),
        P("ep"),
        P("ep", None),
        P("ep", None, "tp"),
        P("ep", None, "tp"),
        P("ep", "tp", None),
        P(None, "tp"),
        P("tp", None),
        P("tp"),
    )
    return jax.shard_map(
        body,
        mesh=mesh,
        in_specs=placed,
        out_specs=(P("ep", "tp"), P("ep", "tp", None), P("ep", "tp", None), P("ep", "tp")),
        check_vma=False,
    )
```

profile of v0, /device:TPU:1, one launch (start us, length us, event | category | flops | bytes accessed | tf_op | source)
XLA Modules:
  0.0 108.0 jit_solution(13230268292263461012)
XLA Ops:
  0.7 21.8 %all_gather.3 = bf16[16,2048]{1,0:T(8,128)(2,1)S(1)} all-gather(bf16[16,128]{1,0:T(8,128)(2,1)} %param.23), channel_id=1, replica_groups=mesh['ep'=16,'tp'=16] {'tp'}, dimensions={1}, use_global_device_ids=true | all-gather | bytes 69632 | tf_op jit(solution)/shard_map/all_gather | solution.py:121
  22.7 1.4 %multiply_reduce_fusion.1 = (f32[16]{0:T(128)S(1)}, f32[16,128]{1,0:T(8,128)S(1)}) fusion(bf16[2048,128]{1,0:T(8,128)(2,1)} %param.30, bf16[16,2048]{1,0:T(8,128)(2,1)S(1)} %all_gather.3, f32[2048]{0:T(1024)} %param.28, f32[16]{0:T(128)S(1)} %add_rsqrt_fusion.3), kind=kOutput, calls=%fused_computation.71 | convolution fusion | flops 8523760 | bytes 606336 | tf_op jit(solution)/shard_map/dot_general | solution.py:128
  24.1 1.4 %multiply_reduce_fusion.2 = (f32[16]{0:T(128)S(1)}, f32[16,128]{1,0:T(8,128)S(1)}) fusion(bf16[2048,128]{1,0:T(8,128)(2,1)} %param.29, bf16[16,2048]{1,0:T(8,128)(2,1)S(1)} %all_gather.3, f32[2048]{0:T(1024)} %param.28, f32[16]{0:T(128)S(1)} %add_rsqrt_fusion.3), kind=kOutput, calls=%fused_computation.74 | convolution fusion | flops 8523760 | bytes 606336 | tf_op jit(solution)/shard_map/dot_general | solution.py:128
  25.5 0.7 broadcast_add_fusion
  26.2 0.8 fusion.59
  27.0 3.4 %fusion.2 = f32[16,1,1024]{2,1,0:T(1,128)S(1)} fusion(bf16[16,1,1024,128]{3,2,1,0:T(8,128)(2,1)} %param.24, bf16[16,128,1]{1,0,2:T(8,128)(2,1)S(1)} %get-tuple-element.10), kind=kOutput, calls=%fused_computation.2 | convolution fusion | flops 4194304 | bytes 4263936 | tf_op jit(solution)/shard_map/shd,shld->shl/dot_general | solution.py:73
  30.4 0.6 dynamic_slice.7
  31.3 1.6 %fusion.51 = f32[16]{0:T(128)S(1)} fusion(f32[16]{0:T(128)S(1)} %fusion.29, bf16[2048,16]{0,1:T(8,128)(2,1)} %param.32, s32[]{:T(128)S(6)} %select_n.34, f32[]{:T(128)} %bitcast.4, bf16[16,2048]{1,0:T(8,128)(2,1)S(1)} %all_gather.3, f32[2048]{0:T(1024)S(1)} %copy-done.8, f32[16]{0:T(128)S(1)} %add_rsqrt_fusion.3), kind=kOutput, calls=%fused_computation.85 | convolution fusion | flops 196768 | bytes 82628 | tf_op jit(solution)/shard_map/dot_general | solution.py:139
  34.3 3.0 %fusion = f32[16,1,128]{2,1,0:T(1,128)S(1)} fusion(bf16[16,1,1024,128]{3,2,1,0:T(8,128)(2,1)} %param.25, f32[16]{0:T(128)S(1)} %get-tuple-element.12, f32[16,1,1024]{2,1,0:T(1,128)S(1)} %get-tuple-element.7, f32[16]{0:T(128)S(1)} %multiply_maximum_fusion, s32[16]{0:T(128)S(1)} %copy-done.12), kind=kOutput, calls=%fused_computation | convolution fusion | flops 4276224 | bytes 4268224 | tf_op jit(solution)/shard_map/shl,shld->shd/dot_general | solution.py:89
  37.3 0.9 convolution_bitcast_fusion
  38.3 3.8 %all-to-all-start = ((f32[16,16,128]{2,1,0:T(8,128)}), f32[16,16,128]{2,1,0:T(8,128)S(1)}, u32[]{:S(2)}, u32[]{:S(2)}) async-start(f32[16,16,128]{2,1,0:T(8,128)} %convolution_bitcast_fusion), calls=%async_computation | async-start | bytes 262144 | tf_op jit(solution)/shard_map/all_to_all | solution.py:20
  42.5 8.5 %all-to-all-done = f32[16,16,128]{2,1,0:T(8,128)S(1)} async-done(((f32[16,16,128]{2,1,0:T(8,128)}), f32[16,16,128]{2,1,0:T(8,128)S(1)}, u32[]{:S(2)}, u32[]{:S(2)}) %all-to-all-start) | async-done | bytes 131104 | tf_op jit(solution)/shard_map/all_to_all | solution.py:20
  51.0 0.6 broadcast_in_dim.32
  51.6 3.4 %all-to-all-start.1 = ((bf16[16,16,128]{2,1,0:T(8,128)(2,1)}), bf16[16,16,128]{2,1,0:T(8,128)(2,1)S(1)}, u32[]{:S(2)}, u32[]{:S(2)}) async-start(bf16[16,16,128]{2,1,0:T(8,128)(2,1)} %broadcast_in_dim.32), calls=%async_computation.1 | async-start | bytes 131072 | tf_op jit(solution)/shard_map/all_to_all | solution.py:32
  55.3 7.2 %all-to-all-done.1 = bf16[16,16,128]{2,1,0:T(8,128)(2,1)S(1)} async-done(((bf16[16,16,128]{2,1,0:T(8,128)(2,1)}), bf16[16,16,128]{2,1,0:T(8,128)(2,1)S(1)}, u32[]{:S(2)}, u32[]{:S(2)}) %all-to-all-start.1) | async-done | bytes 65568 | tf_op jit(solution)/shard_map/all_to_all | solution.py:32
  62.9 0.7 all_to_all.27
  63.6 6.8 %all-to-all-start.2 = ((bf16[16,2,2052]{2,1,0:T(2,128)(2,1)}), bf16[16,2,2052]{2,1,0:T(2,128)(2,1)S(1)}, u32[]{:S(2)}, u32[]{:S(2)}) async-start(bf16[16,2,2052]{2,1,0:T(2,128)(2,1)} %all_to_all.27), calls=%async_computation.2 | async-start | bytes 278528 | tf_op jit(solution)/shard_map/all_to_all | solution.py:42
  70.4 0.4 fusion.44
  70.8 6.4 %all-to-all-done.2 = bf16[16,2,2052]{2,1,0:T(2,128)(2,1)S(1)} async-done(((bf16[16,2,2052]{2,1,0:T(2,128)(2,1)}), bf16[16,2,2052]{2,1,0:T(2,128)(2,1)S(1)}, u32[]{:S(2)}, u32[]{:S(2)}) %all-to-all-start.2) | async-done | bytes 131360 | tf_op jit(solution)/shard_map/all_to_all | solution.py:42
  78.1 18.6 %all_to_all.39 = f32[16,48,128]{2,1,0:T(8,128)S(1)} all-to-all(f32[16,48,128]{2,1,0:T(8,128)S(1)} %bitcast_bitcast_fusion), channel_id=1, replica_groups=mesh['ep'=16,'tp'=16] {'tp'}, dimensions={0} | all-to-all | bytes 786432 | tf_op jit(solution)/shard_map/all_to_all | solution.py:20
  96.8 0.6 split.15
  97.4 3.5 %all-to-all-start.4 = ((bf16[16,2,128]{2,1,0:T(2,128)(2,1)}), bf16[16,2,128]{2,1,0:T(2,128)(2,1)S(1)}, u32[]{:S(2)}, u32[]{:S(2)}) async-start(bf16[16,2,128]{2,1,0:T(2,128)(2,1)} %bitcast.19), calls=%async_computation.4 | async-start | bytes 16384 | tf_op jit(solution)/shard_map/all_to_all | solution.py:189
  100.9 6.3 %all-to-all-done.4 = bf16[16,2,128]{2,1,0:T(2,128)(2,1)S(1)} async-done(((bf16[16,2,128]{2,1,0:T(2,128)(2,1)}), bf16[16,2,128]{2,1,0:T(2,128)(2,1)S(1)}, u32[]{:S(2)}, u32[]{:S(2)}) %all-to-all-start.4) | async-done | bytes 8224 | tf_op jit(solution)/shard_map/all_to_all | solution.py:189
  107.3 0.8 fusion.8
  (74 shorter events, 3.7 us)
Async XLA Ops:
  0.6 77.0 %copy-start = (bf16[1,128,2048]{2,1,0:T(8,128)(2,1)S(1)}, bf16[1,128,2048]{2,1,0:T(8,128)(2,1)}, u32[]{:S(2)}) copy-start(bf16[1,128,2048]{2,1,0:T(8,128)(2,1)} %param.42) | copy-start | bytes 1572868
  0.6 30.7 %copy-start.8 = (f32[2048]{0:T(1024)S(1)}, f32[2048]{0:T(1024)}, u32[]{:S(2)}) copy-start(f32[2048]{0:T(1024)} %param.28) | copy-start | bytes 24580
  0.7 32.4 %copy-start.12 = (s32[16]{0:T(128)S(1)}, s32[16]{0:T(128)}, u32[]{:S(2)}) copy-start(s32[16]{0:T(128)} %param.27) | copy-start | bytes 196
  0.7 29.7 %copy-start.18 = (f32[16]{0:T(128)S(1)}, f32[16]{0:T(128)}, u32[]{:S(2)}) copy-start(f32[16]{0:T(128)} %param.33) | copy-start | bytes 196
  0.7 30.3 %copy-start.7 = (f32[16,1,1024]{2,1,0:T(1,128)S(1)}, f32[16,1,1024]{2,1,0:T(1,128)}, u32[]{:S(2)}) copy-start(f32[16,1,1024]{2,1,0:T(1,128)} %param.26) | copy-start | bytes 196612
  0.7 33.0 %copy-start.1 = (bf16[2048,128]{1,0:T(8,128)(2,1)S(1)}, bf16[2048,128]{1,0:T(8,128)(2,1)}, u32[]{:S(2)}) copy-start(bf16[2048,128]{1,0:T(8,128)(2,1)} %param.31) | copy-start | bytes 1572868
  0.7 33.3 %copy-start.2 = (bf16[128,2048]{1,0:T(8,128)(2,1)S(1)}, bf16[128,2048]{1,0:T(8,128)(2,1)}, u32[]{:S(2)}) copy-start(bf16[128,2048]{1,0:T(8,128)(2,1)} %param.34) | copy-start | bytes 1572868
  30.4 11.7 %copy-start.13 = (s32[16,1]{0,1:T(1,128)S(1)}, s32[16,1]{0,1:T(1,128)}, u32[]{:S(2)}) copy-start(s32[16,1]{0,1:T(1,128)} %param.36) | copy-start | bytes 196
  30.4 12.0 %copy-start.15 = (f32[16,2]{0,1:T(2,128)S(1)}, f32[16,2]{0,1:T(2,128)}, u32[]{:S(2)}) copy-start(f32[16,2]{0,1:T(2,128)} %param.39) | copy-start | bytes 388
  30.4 12.0 %copy-start.17 = (f32[16]{0:T(128)S(1)}, f32[16]{0:T(128)}, u32[]{:S(2)}) copy-start(f32[16]{0:T(128)} %param.38) | copy-start | bytes 196
  30.4 12.1 %copy-start.14 = (s32[16,2]{0,1:T(2,128)S(1)}, s32[16,2]{0,1:T(2,128)}, u32[]{:S(2)}) copy-start(s32[16,2]{0,1:T(2,128)} %param.37) | copy-start | bytes 388
  30.4 20.6 %copy-start.11 = (bf16[16,128]{1,0:T(8,128)(2,1)S(1)}, bf16[16,128]{1,0:T(8,128)(2,1)}, u32[]{:S(2)}) copy-start(bf16[16,128]{1,0:T(8,128)(2,1)} %param.23) | copy-start | bytes 12292
  30.4 32.2 %copy-start.9 = (f32[2048]{0:T(1024)S(1)}, f32[2048]{0:T(1024)}, u32[]{:S(2)}) copy-start(f32[2048]{0:T(1024)} %param.35) | copy-start | bytes 24580
  32.9 29.9 %copy-start.16 = (f32[16]{0:T(128)}, f32[16]{0:T(128)S(1)}, u32[]{:S(2)}) copy-start(f32[16]{0:T(128)S(1)} %fusion.51) | copy-start | bytes 196
  34.0 36.8 %copy-start.10 = (bf16[16,128]{1,0:T(8,128)(2,1)}, bf16[16,128]{1,0:T(8,128)(2,1)S(1)}, u32[]{:S(2)}) copy-start(bf16[16,128]{1,0:T(8,128)(2,1)S(1)} %convolution_convert_fusion.1) | copy-start | bytes 12292
  34.0 36.4 %copy-start.3 = (bf16[128,2048]{1,0:T(8,128)(2,1)S(1)}, bf16[128,2048]{1,0:T(8,128)(2,1)}, u32[]{:S(2)}) copy-start(bf16[128,2048]{1,0:T(8,128)(2,1)} %param.44) | copy-start | bytes 1572868
  34.0 36.4 %copy-start.4 = (bf16[2048,128]{1,0:T(8,128)(2,1)S(1)}, bf16[2048,128]{1,0:T(8,128)(2,1)}, u32[]{:S(2)}) copy-start(bf16[2048,128]{1,0:T(8,128)(2,1)} %param.43) | copy-start | bytes 1572868
  34.3 43.2 %copy-start.5 = (bf16[1,2048,128]{2,1,0:T(8,128)(2,1)S(1)}, bf16[1,2048,128]{2,1,0:T(8,128)(2,1)}, u32[]{:S(2)}) copy-start(bf16[1,2048,128]{2,1,0:T(8,128)(2,1)} %param.40) | copy-start | bytes 1572868
  34.3 43.4 %copy-start.6 = (bf16[1,2048,128]{2,1,0:T(8,128)(2,1)S(1)}, bf16[1,2048,128]{2,1,0:T(8,128)(2,1)}, u32[]{:S(2)}) copy-start(bf16[1,2048,128]{2,1,0:T(8,128)(2,1)} %param.41) | copy-start | bytes 1572868
  37.3 63.6 %copy-start.19 = (f32[128]{0:T(128)S(1)}, f32[128]{0:T(128)}, u32[]{:S(2)}) copy-start(f32[128]{0:T(128)} %param.45) | copy-start | bytes 1540
  38.3 12.7 %all-to-all-start = ((f32[16,16,128]{2,1,0:T(8,128)}), f32[16,16,128]{2,1,0:T(8,128)S(1)}, u32[]{:S(2)}, u32[]{:S(2)}) async-start(f32[16,16,128]{2,1,0:T(8,128)} %convolution_bitcast_fusion), calls=%async_computation | async-start | bytes 262144 | tf_op jit(solution)/shard_map/all_to_all | solution.py:20
  51.6 10.9 %all-to-all-start.1 = ((bf16[16,16,128]{2,1,0:T(8,128)(2,1)}), bf16[16,16,128]{2,1,0:T(8,128)(2,1)S(1)}, u32[]{:S(2)}, u32[]{:S(2)}) async-start(bf16[16,16,128]{2,1,0:T(8,128)(2,1)} %broadcast_in_dim.32), calls=%async_computation.1 | async-start | bytes 131072 | tf_op jit(solution)/shard_map/all_to_all | solution.py:32
  63.6 13.6 %all-to-all-start.2 = ((bf16[16,2,2052]{2,1,0:T(2,128)(2,1)}), bf16[16,2,2052]{2,1,0:T(2,128)(2,1)S(1)}, u32[]{:S(2)}, u32[]{:S(2)}) async-start(bf16[16,2,2052]{2,1,0:T(2,128)(2,1)} %all_to_all.27), calls=%async_computation.2 | async-start | bytes 278528 | tf_op jit(solution)/shard_map/all_to_all | solution.py:42
  97.4 9.9 %all-to-all-start.4 = ((bf16[16,2,128]{2,1,0:T(2,128)(2,1)}), bf16[16,2,128]{2,1,0:T(2,128)(2,1)S(1)}, u32[]{:S(2)}, u32[]{:S(2)}) async-start(bf16[16,2,128]{2,1,0:T(2,128)(2,1)} %bitcast.19), calls=%async_computation.4 | async-start | bytes 16384 | tf_op jit(solution)/shard_map/all_to_all | solution.py:189
where the time goes:
time: 109 us; the launch traced here: 108 us
  blocking collectives  40.5 us (37%)
  waiting for transfers between devices  28.5 us (26%)
  starting transfers between devices  17.4 us (16%)
  matrix products  14.1 us (13%)
  other arithmetic  3.35 us (3%)
  local copies, waits for them, and re-layouts  3.12 us (3%)
    all_gather x1, blocking collectives, body(): gathered = lax.all_gather(tokens, 'tp', axis=1, tiled=True)  21.8 us
    all_to_all x1, blocking collectives, sum_at_owner(): pieces = lax.all_to_all(split_up(array, dim, size), axis, 0, 0, tiled=True)  18.6 us
    all_to_all x1, waiting for transfers between devices, sum_at_owner(): pieces = lax.all_to_all(split_up(array, dim, size), axis, 0, 0, tiled=True)  8.5 us
    all_to_all x1, waiting for transfers between devices, copy_for_each(): return lax.all_to_all(copies, axis, split_axis=0, concat_axis=0, tiled=True)  7.21 us
    all_to_all x1, starting transfers between devices, side_by_side(): lax.all_to_all(both, axis, split_axis=split_dim, concat_axis=concat_dim,...  6.75 us
    all_to_all x1, waiting for transfers between devices, side_by_side(): lax.all_to_all(both, axis, split_axis=split_dim, concat_axis=concat_dim,...  6.44 us
    all_to_all x1, waiting for transfers between devices, body(): lax.all_to_all(expert_sum.astype(jnp.bfloat16), 'ep', split_axis=0, conca...  6.35 us
    all_to_all x1, starting transfers between devices, sum_at_owner(): pieces = lax.all_to_all(split_up(array, dim, size), axis, 0, 0, tiled=True)  3.81 us
  transfers between devices with their start and end apart: 4, of which 4 were waited for; matrix products, arithmetic and copies ran while one was open for 1% of the time, Pallas kernels for 0%

commit v1 on v0

--- a/solution.py
+++ b/solution.py
@@ -118,7 +118,9 @@
     w_dense_out,
     dense_gate,
 ):
-    gathered = lax.all_gather(tokens, "tp", axis=1, tiled=True)
+    gathered = jnp.concatenate(
+        lax.all_to_all(jnp.stack([tokens] * lax.axis_size("tp")), "tp", 0, 0), axis=1
+    )
     normed = norm_rows(gathered, attn_gain)
     seq_count = gathered.shape[0]
     heads_dev = key_cache.shape[1]

time: 109 us -> 105 us (0.963)
  blocking collectives: 40.5 us -> 18.6 us
  starting transfers between devices: 17.4 us -> 30.5 us
  other arithmetic: 3.35 us -> 6.91 us
  local copies, waits for them, and re-layouts: 3.12 us -> 6.18 us
  matrix products: 14.1 us -> 12.1 us
    all_gather x1 -> x0, blocking collectives: 21.8 us -> none  [body(): gathered = lax.all_gather(tokens, 'tp', axis=1, tiled=True)]
    all_to_all x0 -> x1, starting transfers between devices: none -> 9.97 us  [body(): lax.all_to_all(jnp.stack([tokens] * lax.axis_size('tp')), 'tp', 0, 0)]
    all_to_all x1, starting transfers between devices: 3.81 us -> 6.86 us  [sum_at_owner(): pieces = lax.all_to_all(split_up(array, dim, size), axis, 0, 0, tiled=True)]
    dot_general x1, matrix products: 2.99 us -> 0.72 us  [attend(): jnp.einsum('shl,shld->shd', weights, value_cache, preferred_element_type=...]
    another operation x0 -> x1, local copies, waits for them, and re-layouts: none -> 1.38 us  [body(): jnp.stack([tokens] * lax.axis_size('tp'))]
  transfers between devices with their start and end apart: 4 -> 5, of which waited for: 4 -> 5; matrix products, arithmetic and copies ran while one was open for 1% -> 8% of each run, Pallas kernels for 0% -> 0%
where the time goes in v1:
time: 105 us
  starting transfers between devices  30.5 us (29%)
  waiting for transfers between devices  29.2 us (28%)
  blocking collectives  18.6 us (18%)
  matrix products  12.1 us (12%)
  other arithmetic  6.91 us (7%)
  local copies, waits for them, and re-layouts  6.18 us (6%)
    all_to_all x1, blocking collectives, sum_at_owner(): pieces = lax.all_to_all(split_up(array, dim, size), axis, 0, 0, tiled=True)  18.6 us
    all_to_all x1, starting transfers between devices, body(): lax.all_to_all(jnp.stack([tokens] * lax.axis_size('tp')), 'tp', 0, 0)  9.97 us
    all_to_all x1, waiting for transfers between devices, sum_at_owner(): pieces = lax.all_to_all(split_up(array, dim, size), axis, 0, 0, tiled=True)  8.84 us
    all_to_all x1, waiting for transfers between devices, copy_for_each(): return lax.all_to_all(copies, axis, split_axis=0, concat_axis=0, tiled=True)  7.21 us
    all_to_all x1, starting transfers between devices, sum_at_owner(): pieces = lax.all_to_all(split_up(array, dim, size), axis, 0, 0, tiled=True)  6.86 us
    all_to_all x1, starting transfers between devices, side_by_side(): lax.all_to_all(both, axis, split_axis=split_dim, concat_axis=concat_dim,...  6.75 us
    all_to_all x1, waiting for transfers between devices, side_by_side(): lax.all_to_all(both, axis, split_axis=split_dim, concat_axis=concat_dim,...  6.44 us
    all_to_all x1, waiting for transfers between devices, body(): lax.all_to_all(expert_sum.astype(jnp.bfloat16), 'ep', split_axis=0, conca...  6.35 us
  transfers between devices with their start and end apart: 5, of which 5 were waited for; matrix products, arithmetic and copies ran while one was open for 8% of the time, Pallas kernels for 0%

profile of v1, /device:TPU:1, one launch (start us, length us, event | category | flops | bytes accessed | tf_op | source)
XLA Modules:
  0.0 104.5 jit_solution(7083762711332940347)
XLA Ops:
  0.7 1.4 %stack.4 = bf16[16,16,128]{2,1,0:T(8,128)(2,1)} broadcast(bf16[16,128]{1,0:T(8,128)(2,1)} %param.23), dimensions={1,2} | broadcast | bytes 69632 | tf_op jit(solution)/shard_map/stack | solution.py:122
  2.1 10.0 %all-to-all-start = ((bf16[16,16,128]{2,1,0:T(8,128)(2,1)}), bf16[16,16,128]{2,1,0:T(8,128)(2,1)S(1)}, u32[]{:S(2)}, u32[]{:S(2)}) async-start(bf16[16,16,128]{2,1,0:T(8,128)(2,1)} %stack.4), calls=%async_computation | async-start | bytes 131072 | tf_op jit(solution)/shard_map/all_to_all | solution.py:122
  12.7 1.3 %copy.59 = bf16[2048,128]{1,0:T(8,128)(2,1)S(1)} copy(bf16[2048,128]{0,1:T(8,128)(2,1)} %bitcast.129) | data formatting | bytes 1048576 | tf_op jit(solution)/shard_map/dot_general | solution.py:149
  14.0 0.7 fusion.47
  14.8 0.8 select_reduce_fusion.1
  15.6 0.8 broadcast_subtract_fusion
  16.4 1.2 %dynamic_slice.7 = f32[1]{0:T(128)} dynamic-slice(f32[16]{0:T(128)} %param.33, s32[]{:T(128)S(6)} %select_n.34), dynamic_slice_sizes={1} | dynamic-slice | bytes 12 | tf_op jit(solution)/shard_map/dynamic_slice | solution.py:139
  18.3 1.1 %fusion.34 = f32[16]{0:T(128)S(1)} fusion(f32[16,1,1024]{2,1,0:T(1,128)} %param.26, s32[16]{0:T(128)S(1)} %broadcast_add_fusion), kind=kLoop, calls=%fused_computation.53 | loop fusion | flops 49136 | bytes 65664 | tf_op jit(solution)/shard_map/reduce_sum | solution.py:145
  19.9 1.6 %multiply_reduce_fusion.1 = (f32[16]{0:T(128)S(1)}, f32[16,128]{1,0:T(8,128)S(1)}) fusion(bf16[2048,128]{1,0:T(8,128)(2,1)} %param.30, f32[2048]{0:T(1024)} %param.28, f32[16]{0:T(128)S(1)} %add_rsqrt_fusion.3, bf16[16,16,128]{2,1,0:T(8,128)(2,1)S(1)} %all-to-all-done), kind=kOutput, calls=%fused_computation.78 | convolution fusion | flops 8523760 | bytes 606336 | tf_op jit(solution)/shard_map/dot_general | solution.py:130
  21.5 1.4 %multiply_reduce_fusion.2 = (f32[16]{0:T(128)S(1)}, f32[16,128]{1,0:T(8,128)S(1)}) fusion(bf16[2048,128]{1,0:T(8,128)(2,1)} %param.29, f32[2048]{0:T(1024)} %param.28, f32[16]{0:T(128)S(1)} %add_rsqrt_fusion.3, bf16[16,16,128]{2,1,0:T(8,128)(2,1)S(1)} %all-to-all-done), kind=kOutput, calls=%fused_computation.81 | convolution fusion | flops 8523760 | bytes 606336 | tf_op jit(solution)/shard_map/dot_general | solution.py:130
  22.9 0.8 fusion.66
  23.7 3.4 %fusion.2 = f32[16,1,1024]{2,1,0:T(1,128)S(1)} fusion(bf16[16,1,1024,128]{3,2,1,0:T(8,128)(2,1)} %param.24, bf16[16,128,1]{1,0,2:T(8,128)(2,1)S(1)} %get-tuple-element.10), kind=kOutput, calls=%fused_computation.2 | convolution fusion | flops 4194304 | bytes 4263936 | tf_op jit(solution)/shard_map/shd,shld->shl/dot_general | solution.py:73
  27.2 1.7 %fusion.56 = f32[16]{0:T(128)S(1)} fusion(f32[16]{0:T(128)S(1)} %fusion.34, bf16[2048,16]{0,1:T(8,128)(2,1)} %param.32, s32[]{:T(128)S(6)} %select_n.34, f32[]{:T(128)} %bitcast.7, bf16[16,16,128]{2,1,0:T(8,128)(2,1)S(1)} %all-to-all-done, f32[16,128]{1,0:T(8,128)S(1)} %bitcast.130, f32[16]{0:T(128)S(1)} %add_rsqrt_fusion.3), kind=kOutput, calls=%fused_computation.92 | convolution fusion | flops 196768 | bytes 82628 | tf_op jit(solution)/shard_map/dot_general | solution.py:141
  30.7 0.9 convolution_bitcast_fusion
  31.7 6.9 %all-to-all-start.1 = ((f32[16,16,128]{2,1,0:T(8,128)}), f32[16,16,128]{2,1,0:T(8,128)S(1)}, u32[]{:S(2)}, u32[]{:S(2)}) async-start(f32[16,16,128]{2,1,0:T(8,128)} %convolution_bitcast_fusion), calls=%async_computation.1 | async-start | bytes 262144 | tf_op jit(solution)/shard_map/all_to_all | solution.py:20
  38.6 8.8 %all-to-all-done.1 = f32[16,16,128]{2,1,0:T(8,128)S(1)} async-done(((f32[16,16,128]{2,1,0:T(8,128)}), f32[16,16,128]{2,1,0:T(8,128)S(1)}, u32[]{:S(2)}, u32[]{:S(2)}) %all-to-all-start.1) | async-done | bytes 131104 | tf_op jit(solution)/shard_map/all_to_all | solution.py:20
  48.1 3.4 %all-to-all-start.2 = ((bf16[16,16,128]{2,1,0:T(8,128)(2,1)}), bf16[16,16,128]{2,1,0:T(8,128)(2,1)S(1)}, u32[]{:S(2)}, u32[]{:S(2)}) async-start(bf16[16,16,128]{2,1,0:T(8,128)(2,1)} %broadcast_in_dim.32), calls=%async_computation.2 | async-start | bytes 131072 | tf_op jit(solution)/shard_map/all_to_all | solution.py:32
  51.7 7.2 %all-to-all-done.2 = bf16[16,16,128]{2,1,0:T(8,128)(2,1)S(1)} async-done(((bf16[16,16,128]{2,1,0:T(8,128)(2,1)}), bf16[16,16,128]{2,1,0:T(8,128)(2,1)S(1)}, u32[]{:S(2)}, u32[]{:S(2)}) %all-to-all-start.2) | async-done | bytes 65568 | tf_op jit(solution)/shard_map/all_to_all | solution.py:32
  60.0 6.8 %all-to-all-start.3 = ((bf16[16,2,2052]{2,1,0:T(2,128)(2,1)}), bf16[16,2,2052]{2,1,0:T(2,128)(2,1)S(1)}, u32[]{:S(2)}, u32[]{:S(2)}) async-start(bf16[16,2,2052]{2,1,0:T(2,128)(2,1)} %all_to_all.31), calls=%async_computation.3 | async-start | bytes 278528 | tf_op jit(solution)/shard_map/all_to_all | solution.py:42
  67.3 6.4 %all-to-all-done.3 = bf16[16,2,2052]{2,1,0:T(2,128)(2,1)S(1)} async-done(((bf16[16,2,2052]{2,1,0:T(2,128)(2,1)}), bf16[16,2,2052]{2,1,0:T(2,128)(2,1)S(1)}, u32[]{:S(2)}, u32[]{:S(2)}) %all-to-all-start.3) | async-done | bytes 131360 | tf_op jit(solution)/shard_map/all_to_all | solution.py:42
  74.6 18.6 %all_to_all.44 = f32[16,48,128]{2,1,0:T(8,128)S(1)} all-to-all(f32[16,48,128]{2,1,0:T(8,128)S(1)} %bitcast_bitcast_fusion), channel_id=1, replica_groups=mesh['ep'=16,'tp'=16] {'tp'}, dimensions={0} | all-to-all | bytes 786432 | tf_op jit(solution)/shard_map/all_to_all | solution.py:20
  93.8 3.5 %all-to-all-start.5 = ((bf16[16,2,128]{2,1,0:T(2,128)(2,1)}), bf16[16,2,128]{2,1,0:T(2,128)(2,1)S(1)}, u32[]{:S(2)}, u32[]{:S(2)}) async-start(bf16[16,2,128]{2,1,0:T(2,128)(2,1)} %bitcast.22), calls=%async_computation.5 | async-start | bytes 16384 | tf_op jit(solution)/shard_map/all_to_all | solution.py:191
  97.4 6.3 %all-to-all-done.5 = bf16[16,2,128]{2,1,0:T(2,128)(2,1)S(1)} async-done(((bf16[16,2,128]{2,1,0:T(2,128)(2,1)}), bf16[16,2,128]{2,1,0:T(2,128)(2,1)S(1)}, u32[]{:S(2)}, u32[]{:S(2)}) %all-to-all-start.5) | async-done | bytes 8224 | tf_op jit(solution)/shard_map/all_to_all | solution.py:191
  103.7 0.8 fusion.8
  (70 shorter events, 7.6 us)
Async XLA Ops:
  0.6 73.5 %copy-start = (bf16[1,128,2048]{2,1,0:T(8,128)(2,1)S(1)}, bf16[1,128,2048]{2,1,0:T(8,128)(2,1)}, u32[]{:S(2)}) copy-start(bf16[1,128,2048]{2,1,0:T(8,128)(2,1)} %param.42) | copy-start | bytes 1572868
  0.6 28.4 %copy-start.11 = (s32[16]{0:T(128)S(1)}, s32[16]{0:T(128)}, u32[]{:S(2)}) copy-start(s32[16]{0:T(128)} %param.27) | copy-start | bytes 196
  0.7 28.4 %copy-start.6 = (f32[16,1,1024]{2,1,0:T(1,128)S(1)}, f32[16,1,1024]{2,1,0:T(1,128)}, u32[]{:S(2)}) copy-start(f32[16,1,1024]{2,1,0:T(1,128)} %param.26) | copy-start | bytes 196612
  0.7 26.5 %copy-start.7 = (f32[2048]{0:T(1024)S(1)}, f32[2048]{0:T(1024)}, u32[]{:S(2)}) copy-start(f32[2048]{0:T(1024)} %param.28) | copy-start | bytes 24580
  2.1 17.7 %all-to-all-start = ((bf16[16,16,128]{2,1,0:T(8,128)(2,1)}), bf16[16,16,128]{2,1,0:T(8,128)(2,1)S(1)}, u32[]{:S(2)}, u32[]{:S(2)}) async-start(bf16[16,16,128]{2,1,0:T(8,128)(2,1)} %stack.4), calls=%async_computation | async-start | bytes 131072 | tf_op jit(solution)/shard_map/all_to_all | solution.py:122
  19.8 9.9 %copy-start.15 = (bf16[16,1,1024,128]{3,2,1,0:T(8,128)(2,1)S(1)}, bf16[16,1,1024,128]{3,2,1,0:T(8,128)(2,1)}, u32[]{:S(2)}) copy-start(bf16[16,1,1024,128]{3,2,1,0:T(8,128)(2,1)} %param.25) | copy-start | bytes 12582916
  23.7 6.8 %copy-start.1 = (bf16[2048,128]{1,0:T(8,128)(2,1)S(1)}, bf16[2048,128]{1,0:T(8,128)(2,1)}, u32[]{:S(2)}) copy-start(bf16[2048,128]{1,0:T(8,128)(2,1)} %param.31) | copy-start | bytes 1572868
  27.2 11.4 %copy-start.13 = (s32[16,2]{0,1:T(2,128)S(1)}, s32[16,2]{0,1:T(2,128)}, u32[]{:S(2)}) copy-start(s32[16,2]{0,1:T(2,128)} %param.37) | copy-start | bytes 388
  27.2 11.4 %copy-start.12 = (s32[16,1]{0,1:T(1,128)S(1)}, s32[16,1]{0,1:T(1,128)}, u32[]{:S(2)}) copy-start(s32[16,1]{0,1:T(1,128)} %param.36) | copy-start | bytes 196
  27.2 20.3 %copy-start.10 = (bf16[16,128]{1,0:T(8,128)(2,1)S(1)}, bf16[16,128]{1,0:T(8,128)(2,1)}, u32[]{:S(2)}) copy-start(bf16[16,128]{1,0:T(8,128)(2,1)} %param.23) | copy-start | bytes 12292
  27.2 31.9 %copy-start.8 = (f32[2048]{0:T(1024)S(1)}, f32[2048]{0:T(1024)}, u32[]{:S(2)}) copy-start(f32[2048]{0:T(1024)} %param.35) | copy-start | bytes 24580
  27.2 39.6 %copy-start.2 = (bf16[128,2048]{1,0:T(8,128)(2,1)S(1)}, bf16[128,2048]{1,0:T(8,128)(2,1)}, u32[]{:S(2)}) copy-start(bf16[128,2048]{1,0:T(8,128)(2,1)} %param.44) | copy-start | bytes 1572868
  27.2 39.6 %copy-start.3 = (bf16[2048,128]{1,0:T(8,128)(2,1)S(1)}, bf16[2048,128]{1,0:T(8,128)(2,1)}, u32[]{:S(2)}) copy-start(bf16[2048,128]{1,0:T(8,128)(2,1)} %param.43) | copy-start | bytes 1572868
  28.9 38.3 %copy-start.14 = (f32[16]{0:T(128)}, f32[16]{0:T(128)S(1)}, u32[]{:S(2)}) copy-start(f32[16]{0:T(128)S(1)} %fusion.56) | copy-start | bytes 196
  29.7 44.2 %copy-start.4 = (bf16[1,2048,128]{2,1,0:T(8,128)(2,1)S(1)}, bf16[1,2048,128]{2,1,0:T(8,128)(2,1)}, u32[]{:S(2)}) copy-start(bf16[1,2048,128]{2,1,0:T(8,128)(2,1)} %param.40) | copy-start | bytes 1572868
  29.7 44.4 %copy-start.5 = (bf16[1,2048,128]{2,1,0:T(8,128)(2,1)S(1)}, bf16[1,2048,128]{2,1,0:T(8,128)(2,1)}, u32[]{:S(2)}) copy-start(bf16[1,2048,128]{2,1,0:T(8,128)(2,1)} %param.41) | copy-start | bytes 1572868
  30.7 73.8 %copy-start.9 = (bf16[16,128]{1,0:T(8,128)(2,1)}, bf16[16,128]{1,0:T(8,128)(2,1)S(1)}, u32[]{:S(2)}) copy-start(bf16[16,128]{1,0:T(8,128)(2,1)S(1)} %convolution_convert_fusion.1) | copy-start | bytes 12292
  30.7 66.6 %copy-start.16 = (f32[128]{0:T(128)S(1)}, f32[128]{0:T(128)}, u32[]{:S(2)}) copy-start(f32[128]{0:T(128)} %param.45) | copy-start | bytes 1540
  31.7 15.7 %all-to-all-start.1 = ((f32[16,16,128]{2,1,0:T(8,128)}), f32[16,16,128]{2,1,0:T(8,128)S(1)}, u32[]{:S(2)}, u32[]{:S(2)}) async-start(f32[16,16,128]{2,1,0:T(8,128)} %convolution_bitcast_fusion), calls=%async_computation.1 | async-start | bytes 262144 | tf_op jit(solution)/shard_map/all_to_all | solution.py:20
  48.1 10.9 %all-to-all-start.2 = ((bf16[16,16,128]{2,1,0:T(8,128)(2,1)}), bf16[16,16,128]{2,1,0:T(8,128)(2,1)S(1)}, u32[]{:S(2)}, u32[]{:S(2)}) async-start(bf16[16,16,128]{2,1,0:T(8,128)(2,1)} %broadcast_in_dim.32), calls=%async_computation.2 | async-start | bytes 131072 | tf_op jit(solution)/shard_map/all_to_all | solution.py:32
  60.0 13.6 %all-to-all-start.3 = ((bf16[16,2,2052]{2,1,0:T(2,128)(2,1)}), bf16[16,2,2052]{2,1,0:T(2,128)(2,1)S(1)}, u32[]{:S(2)}, u32[]{:S(2)}) async-start(bf16[16,2,2052]{2,1,0:T(2,128)(2,1)} %all_to_all.31), calls=%async_computation.3 | async-start | bytes 278528 | tf_op jit(solution)/shard_map/all_to_all | solution.py:42
  93.8 9.9 %all-to-all-start.5 = ((bf16[16,2,128]{2,1,0:T(2,128)(2,1)}), bf16[16,2,128]{2,1,0:T(2,128)(2,1)S(1)}, u32[]{:S(2)}, u32[]{:S(2)}) async-start(bf16[16,2,128]{2,1,0:T(2,128)(2,1)} %bitcast.22), calls=%async_computation.5 | async-start | bytes 16384 | tf_op jit(solution)/shard_map/all_to_all | solution.py:191
